TPU v7x, 32 devices: a whole 2x2x4 slice. The times are simulated.
32 devices in a mesh: sp: 4 (over y, x), tp: 8 (over z, core).
Axes of the slice: x: 2, y: 2, z: 4, core: 2. Of those that a mesh axis runs over, the one named last changes fastest.
Arguments:
- stream: bfloat16 [2048, 1024], P('sp', 'tp'), may hold values from -6 to 6
- gain_first: bfloat16 [1024], P('tp'), may hold values from 0.099609375 to 1.8984375
- query_first: bfloat16 [1024, 1024], P('sp', 'tp'), may hold values from -0.1875 to 0.1875
- key_first: bfloat16 [1024, 1024], P('sp', 'tp'), may hold values from -0.1875 to 0.1875
- value_first: bfloat16 [1024, 1024], P('sp', 'tp'), may hold values from -0.1875 to 0.1875
- offset_first: float32 [8, 15, 31], P('tp'), may hold values from -4 to 254
- gain_second: bfloat16 [1024], P('tp'), may hold values from 0.099609375 to 1.8984375
- query_second: bfloat16 [1024, 1024], P('sp', 'tp'), may hold values from -0.1875 to 0.1875
- key_second: bfloat16 [1024, 1024], P('sp', 'tp'), may hold values from -0.1875 to 0.1875
- value_second: bfloat16 [1024, 1024], P('sp', 'tp'), may hold values from -0.1875 to 0.1875
- offset_second: float32 [8, 15, 31], P('tp'), may hold values from -4 to 254
Outputs:
- result: bfloat16 [2048, 1024], P('sp', 'tp')
All inputs are finite; a program needn't handle non-finite values.
Results may differ from a plain program's by a relative error of at most 0.008.
Values may be sent and summed in bfloat16 or wider, within the bound.
A program may use at most 64 MiB of HBM per device.

v0:
```python
import jax
import jax.numpy as jnp
import numpy as np
from jax import lax
from jax.sharding import PartitionSpec as P

GRID_W = 64
epsilon = 1e-06


def padded_2(block, sides, width):
    for axis, dim in sides:
        count = lax.axis_size(axis)
        forward = [(i, i + 1) for i in range(count - 1)]
        backward = [(target, source) for source, target in forward]
        low = lax.ppermute(
            lax.slice_in_dim(block, block.shape[dim] - width, None, axis=dim), axis, forward
        )
        high = lax.ppermute(lax.slice_in_dim(block, 0, width, axis=dim), axis, backward)
        block = jnp.concatenate([low, block, high], axis=dim)
    return block


def attend(query, keys, values, table, row_start, total_rows):
    rows_here, width, heads, head_size = query.shape
    blocks = width // 16
    query_cols = np.arange(width).reshape(blocks, 16)
    window_start = np.clip(query_cols - 8, 0, width - 16)
    key_cols = np.clip(np.arange(blocks) * 16 - 8, 0, width - 32)[:, None] + np.arange(32)
    column_ok = (key_cols[:, None, :] >= window_start[:, :, None]) & (
        key_cols[:, None, :] < window_start[:, :, None] + 16
    )
    column_offset = np.clip(key_cols[:, None, :] - query_cols[:, :, None] + 15, 0, 30)
    column_bias = table[:, :, column_offset]
    mask = jnp.asarray(column_ok)[None, :, :, None, :]
    factor = head_size ** (-0.5)

    def one_row(index):
        grid_row = row_start + index
        first = jnp.clip(grid_row - 4, 0, total_rows - 8)
        local = first - row_start + 4
        key_block = lax.dynamic_slice_in_dim(keys, local, 8, 0)[:, key_cols]
        value_block = lax.dynamic_slice_in_dim(values, local, 8, 0)[:, key_cols]
        query_row = lax.dynamic_index_in_dim(query, index, 0, keepdims=False).reshape(
            blocks, 16, heads, head_size
        )
        scores = (
            jnp.einsum(
                "jqhe,mjkhe->hjqmk", query_row, key_block, preferred_element_type=jnp.float32
            )
            * factor
        )
        row_offset = first + jnp.arange(8, dtype=jnp.int32) - grid_row + 7
        row_bias = jnp.transpose(jnp.take(column_bias, row_offset, axis=1), (0, 2, 3, 1, 4))
        scores = jnp.where(mask, scores + row_bias, -1e30)
        weight = jax.nn.softmax(scores.reshape(heads, blocks, 16, 256), axis=-1)
        rounded = weight.astype(jnp.bfloat16).reshape(heads, blocks, 16, 8, 32)
        output = jnp.einsum(
            "hjqmk,mjkhe->jqhe", rounded, value_block, preferred_element_type=jnp.float32
        )
        return output.reshape(width, heads * head_size)

    return jax.vmap(one_row)(jnp.arange(rows_here, dtype=jnp.int32))


def layer(stream, gain, w_query, w_key, w_value, table):
    tokens_dev, local_width = stream.shape
    widened = stream.astype(jnp.float32)
    full_rows, full_gain = (
        lax.all_gather(stream, "tp", axis=1, tiled=True),
        lax.all_gather(gain, "tp", axis=0, tiled=True),
    )
    full_wide = full_rows.astype(jnp.float32)
    mean_square = jnp.mean(full_wide * full_wide, axis=-1, keepdims=True)
    normed = (full_wide * lax.rsqrt(mean_square + epsilon) * full_gain.astype(jnp.float32)).astype(
        jnp.bfloat16
    )
    pieces = (
        lax.all_gather(w_query, "sp", axis=0, tiled=True),
        lax.all_gather(w_key, "sp", axis=0, tiled=True),
        lax.all_gather(w_value, "sp", axis=0, tiled=True),
    )
    query, key_part, value_part = tuple(
        (jnp.dot(normed, piece, preferred_element_type=jnp.float32) for piece in pieces)
    )
    heads_dev = table.shape[0]
    rows_dev = tokens_dev // GRID_W
    shape = (rows_dev, GRID_W, heads_dev, local_width // heads_dev)
    query = query.astype(jnp.bfloat16).reshape(shape)
    paired = jnp.stack(
        [
            key_part.astype(jnp.bfloat16).reshape(shape),
            value_part.astype(jnp.bfloat16).reshape(shape),
        ]
    )
    padded = padded_2(paired, (("sp", 1),), 4)
    row_start = lax.axis_index("sp") * rows_dev
    output = attend(query, padded[0], padded[1], table, row_start, rows_dev * lax.axis_size("sp"))
    return (widened + output.reshape(tokens_dev, local_width)).astype(jnp.bfloat16)


def body(
    stream,
    gain_first,
    query_first,
    key_first,
    value_first,
    offset_first,
    gain_second,
    query_second,
    key_second,
    value_second,
    offset_second,
):
    middle = layer(stream, gain_first, query_first, key_first, value_first, offset_first)
    return layer(middle, gain_second, query_second, key_second, value_second, offset_second)


def solution(mesh):
    placed = (
        P("sp", "tp"),
        P("tp"),
        P("sp", "tp"),
        P("sp", "tp"),
        P("sp", "tp"),
        P("tp", None, None),
        P("tp"),
        P("sp", "tp"),
        P("sp", "tp"),
        P("sp", "tp"),
        P("tp", None, None),
    )
    return jax.shard_map(body, mesh=mesh, in_specs=placed, out_specs=P("sp", "tp"), check_vma=False)
```

profile of v0, /device:TPU:0, one launch (start us, length us, event | category | flops | bytes accessed | tf_op | source)
XLA Modules:
  0.0 178.0 jit_solution(1198748897134902003)
XLA Ops:
  7.3 13.6 %all-gather = bf16[8,1,128]{2,1,0:T(2,128)(2,1)S(1)} all-gather(bf16[1,1,128]{2,1,0:T(2,128)(2,1)} %bitcast.156), channel_id=1, replica_groups=mesh['sp'=4,'tp'=8] {'tp'}, dimensions={0}, use_global_device_ids=true | all-gather | bytes 2304 | tf_op jit(solution)/shard_map/all_gather | solution.py:71
  22.6 5.5 %gather_fusion.5 = f32[2048,15]{1,0:T(8,128)S(1)} fusion(f32[15,31]{0,1:T(8,128)S(1)} %bitcast.126, s32[2048]{0:T(1024)S(1)} %broadcast_clamp_fusion), kind=kCustom, calls=%fused_computation.7 | custom fusion | bytes 253952 | tf_op jit(solution)/shard_map/gather | solution.py:34
  29.5 9.0 %all_gather.32 = bf16[1024,128]{1,0:T(8,128)(2,1)S(1)} all-gather(bf16[256,128]{1,0:T(8,128)(2,1)S(1)} %copy-done.4), channel_id=1, replica_groups=mesh['sp'=4,'tp'=8] {'sp'}, dimensions={0}, use_global_device_ids=true | all-gather | bytes 327680 | tf_op jit(solution)/shard_map/all_gather | solution.py:80
  38.5 9.0 %all_gather.33 = bf16[1024,128]{1,0:T(8,128)(2,1)S(1)} all-gather(bf16[256,128]{1,0:T(8,128)(2,1)S(1)} %copy-done.5), channel_id=1, replica_groups=mesh['sp'=4,'tp'=8] {'sp'}, dimensions={0}, use_global_device_ids=true | all-gather | bytes 327680 | tf_op jit(solution)/shard_map/all_gather | solution.py:81
  47.5 8.4 %all_gather.34 = bf16[1024,128]{1,0:T(8,128)(2,1)S(1)} all-gather(bf16[256,128]{1,0:T(8,128)(2,1)S(1)} %copy-done.6), channel_id=1, replica_groups=mesh['sp'=4,'tp'=8] {'sp'}, dimensions={0}, use_global_device_ids=true | all-gather | bytes 327680 | tf_op jit(solution)/shard_map/all_gather | solution.py:79
  58.7 1.7 convolution_convert_fusion.5
  61.0 3.0 %collective-permute-start = (bf16[2,4,64,1,128]{4,2,1,3,0:T(8,128)(2,1)S(1)}, bf16[2,4,64,1,128]{4,2,1,3,0:T(8,128)(2,1)S(1)}, u32[]{:S(2)}, u32[]{:S(2)}) collective-permute-start(bf16[2,4,64,1,128]{4,2,1,3,0:T(8,128)(2,1)S(1)} %get-tuple-element.12), channel_id=1, source_target_pairs={{0,8},{8,16},{16,24},{1,9},{9,17},{17,25},{2,10},{10,18},{18,26},{... | collective-permute-start | bytes 393224 | tf_op jit(solution)/shard_map/ppermute | solution.py:16
  66.6 4.4 %collective-permute-done.1 = bf16[2,4,64,1,128]{4,2,1,3,0:T(8,128)(2,1)S(1)} collective-permute-done((bf16[2,4,64,1,128]{4,2,1,3,0:T(8,128)(2,1)S(1)}, bf16[2,4,64,1,128]{4,2,1,3,0:T(8,128)(2,1)S(1)}, u32[]{:S(2)}, u32[]{:S(2)}) %collective-permute-start.1) | collective-permute-done | bytes 131104 | tf_op jit(solution)/shard_map/ppermute | solution.py:19
  71.1 1.7 gather_fusion.3
  72.7 1.9 %copy.56 = bf16[8,8,64,128]{3,1,2,0:T(8,128)(2,1)S(1)} copy(bf16[8,8,64,128]{3,2,1,0:T(8,128)(2,1)} %gather_fusion.3) | data formatting | bytes 2097152 | tf_op jit(solution)/shard_map/vmap()/gather | solution.py:42
  74.6 2.7 %gather_fusion.4 = bf16[128,8,8,128]{3,2,1,0:T(8,128)(2,1)} fusion(bf16[8,8,64,128]{3,1,2,0:T(8,128)(2,1)S(1)} %copy.56, s32[1024]{0:T(1024)} %pad_clamp_fusion.1), kind=kCustom, calls=%fused_computation.6 | custom fusion | bytes 4194816 | tf_op jit(solution)/shard_map/vmap()/gather | solution.py:42
  77.3 4.5 %fusion.39 = (f32[8,4,16]{2,1,0:T(4,128)S(1)}, f32[8,1,4,16,8,32]{5,3,4,2,0,1:T(8,128)S(1)}) fusion(f32[8,1,8,4,16,32]{5,4,3,2,0,1:T(8,128)S(1)} %bitcast.130, pred[8,8]{1,0:T(8,128)(4,1)} %compare_and_fusion, bf16[8,4,16,128,1]{3,2,4,1,0:T(8,128)(2,1)S(1)} %bitcast.139, bf16[4,32,8,8,128]{4,3,2,1,0:T(8,128)(2,1)} %bitcast.135, ...), kind=kOutput, calls=%fused_computation.87 | convolution fusion | flops 34209280 | bytes 3280960 | tf_op jit(solution)/shard_map/vmap(jqhe,mjkhe->hjqmk)/dot_general | solution.py:48
  84.2 1.7 gather_fusion
  85.9 1.9 %copy.52 = bf16[8,8,64,128]{3,1,2,0:T(8,128)(2,1)S(1)} copy(bf16[8,8,64,128]{3,2,1,0:T(8,128)(2,1)} %gather_fusion) | data formatting | bytes 2097152 | tf_op jit(solution)/shard_map/vmap()/gather | solution.py:43
  87.8 2.5 %gather_fusion.1 = bf16[128,8,8,128]{3,2,1,0:T(8,128)(2,1)} fusion(bf16[8,8,64,128]{3,1,2,0:T(8,128)(2,1)S(1)} %copy.52, s32[1024]{0:T(1024)S(1)} %copy-done.10), kind=kCustom, calls=%fused_computation.3 | custom fusion | bytes 4194816 | tf_op jit(solution)/shard_map/vmap()/gather | solution.py:43
  90.4 2.4 %fusion.14 = f32[8,4,128,16,1]{2,3,4,1,0:T(8,128)S(1)} fusion(bf16[8,4,16,8,32]{2,3,4,1,0:T(8,128)(2,1)S(1)} %copy.61, bf16[4,32,8,8,128]{4,3,2,1,0:T(8,128)(2,1)} %bitcast.133), kind=kOutput, calls=%fused_computation.34 | convolution fusion | flops 33554432 | bytes 2621440 | tf_op jit(solution)/shard_map/vmap(hjqmk,mjkhe->jqhe)/dot_general | solution.py:58
  93.6 8.6 %all-gather.1 = bf16[8,1,128]{2,1,0:T(2,128)(2,1)S(1)} all-gather(bf16[1,1,128]{2,1,0:T(2,128)(2,1)S(1)} %bitcast.157), channel_id=1, replica_groups=mesh['sp'=4,'tp'=8] {'tp'}, dimensions={0}, use_global_device_ids=true | all-gather | bytes 2304 | tf_op jit(solution)/shard_map/all_gather | solution.py:71
  102.3 5.5 %gather_fusion.11 = f32[2048,15]{1,0:T(8,128)S(1)} fusion(f32[15,31]{0,1:T(8,128)S(1)} %bitcast.127, s32[2048]{0:T(1024)S(1)} %broadcast_clamp_fusion), kind=kCustom, calls=%fused_computation.13 | custom fusion | bytes 253952 | tf_op jit(solution)/shard_map/gather | solution.py:34
  109.2 9.8 %all_gather.38 = bf16[1024,128]{1,0:T(8,128)(2,1)S(1)} all-gather(bf16[256,128]{1,0:T(8,128)(2,1)S(1)} %copy-done.7), channel_id=1, replica_groups=mesh['sp'=4,'tp'=8] {'sp'}, dimensions={0}, use_global_device_ids=true | all-gather | bytes 327680 | tf_op jit(solution)/shard_map/all_gather | solution.py:81
  119.0 7.5 %all_gather.37 = bf16[1024,128]{1,0:T(8,128)(2,1)S(1)} all-gather(bf16[256,128]{1,0:T(8,128)(2,1)S(1)} %copy-done.8), channel_id=1, replica_groups=mesh['sp'=4,'tp'=8] {'sp'}, dimensions={0}, use_global_device_ids=true | all-gather | bytes 327680 | tf_op jit(solution)/shard_map/all_gather | solution.py:80
  126.5 9.5 %all_gather.39 = bf16[1024,128]{1,0:T(8,128)(2,1)S(1)} all-gather(bf16[256,128]{1,0:T(8,128)(2,1)S(1)} %copy-done.9), channel_id=1, replica_groups=mesh['sp'=4,'tp'=8] {'sp'}, dimensions={0}, use_global_device_ids=true | all-gather | bytes 327680 | tf_op jit(solution)/shard_map/all_gather | solution.py:79
  137.6 1.7 convolution_convert_fusion.1
  139.9 1.9 %collective-permute-start.2 = (bf16[2,4,64,1,128]{4,2,1,3,0:T(8,128)(2,1)S(1)}, bf16[2,4,64,1,128]{4,2,1,3,0:T(8,128)(2,1)S(1)}, u32[]{:S(2)}, u32[]{:S(2)}) collective-permute-start(bf16[2,4,64,1,128]{4,2,1,3,0:T(8,128)(2,1)S(1)} %get-tuple-element.10), channel_id=1, source_target_pairs={{0,8},{8,16},{16,24},{1,9},{9,17},{17,25},{2,10},{10,18},{18,26},{... | collective-permute-start | bytes 393224 | tf_op jit(solution)/shard_map/ppermute | solution.py:16
  144.3 4.4 %collective-permute-done.3 = bf16[2,4,64,1,128]{4,2,1,3,0:T(8,128)(2,1)S(1)} collective-permute-done((bf16[2,4,64,1,128]{4,2,1,3,0:T(8,128)(2,1)S(1)}, bf16[2,4,64,1,128]{4,2,1,3,0:T(8,128)(2,1)S(1)}, u32[]{:S(2)}, u32[]{:S(2)}) %collective-permute-start.3) | collective-permute-done | bytes 131104 | tf_op jit(solution)/shard_map/ppermute | solution.py:19
  148.8 1.7 gather_fusion.9
  150.5 1.9 %copy.66 = bf16[8,8,64,128]{3,1,2,0:T(8,128)(2,1)S(1)} copy(bf16[8,8,64,128]{3,2,1,0:T(8,128)(2,1)} %gather_fusion.9) | data formatting | bytes 2097152 | tf_op jit(solution)/shard_map/vmap()/gather | solution.py:42
  152.4 2.5 %gather_fusion.10 = bf16[128,8,8,128]{3,2,1,0:T(8,128)(2,1)} fusion(bf16[8,8,64,128]{3,1,2,0:T(8,128)(2,1)S(1)} %copy.66, s32[1024]{0:T(1024)S(1)} %copy-done.11), kind=kCustom, calls=%fused_computation.12 | custom fusion | bytes 4194816 | tf_op jit(solution)/shard_map/vmap()/gather | solution.py:42
  154.9 4.5 %fusion.40 = (f32[8,4,16]{2,1,0:T(4,128)S(1)}, f32[8,1,4,16,8,32]{5,3,4,2,0,1:T(8,128)S(1)}) fusion(f32[8,1,8,4,16,32]{5,4,3,2,0,1:T(8,128)S(1)} %bitcast.131, pred[8,8]{1,0:T(8,128)(4,1)S(1)} %copy-done.14, bf16[8,4,16,128,1]{3,2,4,1,0:T(8,128)(2,1)S(1)} %bitcast.138, bf16[4,32,8,8,128]{4,3,2,1,0:T(8,128)(2,1)} %bitcast.134, ...), kind=kOutput, calls=%fused_computation.88 | convolution fusion | flops 34209280 | bytes 3280960 | tf_op jit(solution)/shard_map/vmap(jqhe,mjkhe->hjqmk)/dot_general | solution.py:48
  161.9 1.7 gather_fusion.6
  163.5 1.9 %copy.62 = bf16[8,8,64,128]{3,1,2,0:T(8,128)(2,1)S(1)} copy(bf16[8,8,64,128]{3,2,1,0:T(8,128)(2,1)} %gather_fusion.6) | data formatting | bytes 2097152 | tf_op jit(solution)/shard_map/vmap()/gather | solution.py:43
  165.4 2.5 %gather_fusion.7 = bf16[128,8,8,128]{3,2,1,0:T(8,128)(2,1)} fusion(bf16[8,8,64,128]{3,1,2,0:T(8,128)(2,1)S(1)} %copy.62, s32[1024]{0:T(1024)S(1)} %copy-done.11), kind=kCustom, calls=%fused_computation.9 | custom fusion | bytes 4194816 | tf_op jit(solution)/shard_map/vmap()/gather | solution.py:43
  168.0 2.4 %fusion.9 = f32[8,4,128,16,1]{2,3,4,1,0:T(8,128)S(1)} fusion(bf16[8,4,16,8,32]{2,3,4,1,0:T(8,128)(2,1)S(1)} %copy.71, bf16[4,32,8,8,128]{4,3,2,1,0:T(8,128)(2,1)} %bitcast.132), kind=kOutput, calls=%fused_computation.28 | convolution fusion | flops 33554432 | bytes 2621440 | tf_op jit(solution)/shard_map/vmap(hjqmk,mjkhe->jqhe)/dot_general | solution.py:58
  (87 shorter events, 22.2 us)
Async XLA Ops:
  6.5 50.6 %all-gather.5.cloned.1.call-start = ((), (), s32[]{:S(2)}) async-start(), calls=%async_computation | async-start | bytes 1179648 | tf_op jit(solution)/shard_map/all_gather | solution.py:70
  7.3 128.7 %all-gather.7.cloned.1.call-start = ((), (), s32[]{:S(2)}) async-start(), calls=%async_computation.1 | async-start | bytes 1179648 | tf_op jit(solution)/shard_map/all_gather | solution.py:70
  28.7 0.8 copy-start.12
  28.7 0.8 copy-start.4
  28.7 9.8 %copy-start.5 = (bf16[256,128]{1,0:T(8,128)(2,1)S(1)}, bf16[256,128]{1,0:T(8,128)(2,1)}, u32[]{:S(2)}) copy-start(bf16[256,128]{1,0:T(8,128)(2,1)} %param.29) | copy-start | bytes 196612
  28.7 18.8 %copy-start.6 = (bf16[256,128]{1,0:T(8,128)(2,1)S(1)}, bf16[256,128]{1,0:T(8,128)(2,1)}, u32[]{:S(2)}) copy-start(bf16[256,128]{1,0:T(8,128)(2,1)} %param.27) | copy-start | bytes 196612
  28.7 27.1 %copy-start.17 = (s32[128]{0:T(128)S(1)}, s32[128]{0:T(128)}, u32[]{:S(2)}) copy-start(s32[128]{0:T(128)} %constant.239) | copy-start | bytes 1540
  57.1 3.3 %copy-start.1 = (bf16[512,1024]{1,0:T(8,128)(2,1)S(1)}, bf16[512,1024]{1,0:T(8,128)(2,1)}, u32[]{:S(2)}) copy-start(bf16[512,1024]{1,0:T(8,128)(2,1)} %all-gather.5.cloned.1.call-done) | copy-start | bytes 3145732
  61.0 5.6 %collective-permute-start = (bf16[2,4,64,1,128]{4,2,1,3,0:T(8,128)(2,1)S(1)}, bf16[2,4,64,1,128]{4,2,1,3,0:T(8,128)(2,1)S(1)}, u32[]{:S(2)}, u32[]{:S(2)}) collective-permute-start(bf16[2,4,64,1,128]{4,2,1,3,0:T(8,128)(2,1)S(1)} %get-tuple-element.12), channel_id=1, source_target_pairs={{0,8},{8,16},{16,24},{1,9},{9,17},{17,25},{2,10},{10,18},{18,26},{... | collective-permute-start | bytes 393224 | tf_op jit(solution)/shard_map/ppermute | solution.py:16
  64.1 6.9 %collective-permute-start.1 = (bf16[2,4,64,1,128]{4,2,1,3,0:T(8,128)(2,1)S(1)}, bf16[2,4,64,1,128]{4,2,1,3,0:T(8,128)(2,1)S(1)}, u32[]{:S(2)}, u32[]{:S(2)}) collective-permute-start(bf16[2,4,64,1,128]{4,2,1,3,0:T(8,128)(2,1)S(1)} %get-tuple-element.13), channel_id=1, source_target_pairs={{8,0},{16,8},{24,16},{9,1},{17,9},{25,17},{10,2},{18,10},{26,18},{... | collective-permute-start | bytes 393224 | tf_op jit(solution)/shard_map/ppermute | solution.py:19
  84.2 3.6 %copy-start.10 = (s32[1024]{0:T(1024)S(1)}, s32[1024]{0:T(1024)}, u32[]{:S(2)}) copy-start(s32[1024]{0:T(1024)} %pad_clamp_fusion.1) | copy-start | bytes 12292
  90.4 2.4 %copy-start.3 = (bf16[512,128]{1,0:T(8,128)(2,1)S(1)}, bf16[512,128]{1,0:T(8,128)(2,1)}, u32[]{:S(2)}) copy-start(bf16[512,128]{1,0:T(8,128)(2,1)} %param.25) | copy-start | bytes 393220
  90.4 3.2 %copy-start.16 = (bf16[128]{0:T(256)(128)(2,1)S(1)}, bf16[128]{0:T(256)(128)(2,1)}, u32[]{:S(2)}) copy-start(bf16[128]{0:T(256)(128)(2,1)} %param.31) | copy-start | bytes 772
  90.4 11.8 %copy-start.15 = (f32[1,15,31]{2,0,1:T(1,128)S(1)}, f32[1,15,31]{2,0,1:T(1,128)}, u32[]{:S(2)}) copy-start(f32[1,15,31]{2,0,1:T(1,128)} %param.35) | copy-start | bytes 5584
  102.3 6.1 %copy-start.13 = (s32[1024]{0:T(1024)S(1)}, s32[1024]{0:T(1024)}, u32[]{:S(2)}) copy-start(s32[1024]{0:T(1024)} %copy-done.12) | copy-start | bytes 12292
  108.4 0.8 copy-start.7
  108.4 10.7 %copy-start.8 = (bf16[256,128]{1,0:T(8,128)(2,1)S(1)}, bf16[256,128]{1,0:T(8,128)(2,1)}, u32[]{:S(2)}) copy-start(bf16[256,128]{1,0:T(8,128)(2,1)} %param.33) | copy-start | bytes 196612
  108.4 18.1 %copy-start.9 = (bf16[256,128]{1,0:T(8,128)(2,1)S(1)}, bf16[256,128]{1,0:T(8,128)(2,1)}, u32[]{:S(2)}) copy-start(bf16[256,128]{1,0:T(8,128)(2,1)} %param.32) | copy-start | bytes 196612
  136.0 3.3 %copy-start.2 = (bf16[512,1024]{1,0:T(8,128)(2,1)S(1)}, bf16[512,1024]{1,0:T(8,128)(2,1)}, u32[]{:S(2)}) copy-start(bf16[512,1024]{1,0:T(8,128)(2,1)} %all-gather.7.cloned.1.call-done) | copy-start | bytes 3145732
  139.9 4.4 %collective-permute-start.2 = (bf16[2,4,64,1,128]{4,2,1,3,0:T(8,128)(2,1)S(1)}, bf16[2,4,64,1,128]{4,2,1,3,0:T(8,128)(2,1)S(1)}, u32[]{:S(2)}, u32[]{:S(2)}) collective-permute-start(bf16[2,4,64,1,128]{4,2,1,3,0:T(8,128)(2,1)S(1)} %get-tuple-element.10), channel_id=1, source_target_pairs={{0,8},{8,16},{16,24},{1,9},{9,17},{17,25},{2,10},{10,18},{18,26},{... | collective-permute-start | bytes 393224 | tf_op jit(solution)/shard_map/ppermute | solution.py:16
  141.8 6.9 %collective-permute-start.3 = (bf16[2,4,64,1,128]{4,2,1,3,0:T(8,128)(2,1)S(1)}, bf16[2,4,64,1,128]{4,2,1,3,0:T(8,128)(2,1)S(1)}, u32[]{:S(2)}, u32[]{:S(2)}) collective-permute-start(bf16[2,4,64,1,128]{4,2,1,3,0:T(8,128)(2,1)S(1)} %get-tuple-element.11), channel_id=1, source_target_pairs={{8,0},{16,8},{24,16},{9,1},{17,9},{25,17},{10,2},{18,10},{26,18},{... | collective-permute-start | bytes 393224 | tf_op jit(solution)/shard_map/ppermute | solution.py:19
  148.8 3.6 %copy-start.11 = (s32[1024]{0:T(1024)S(1)}, s32[1024]{0:T(1024)}, u32[]{:S(2)}) copy-start(s32[1024]{0:T(1024)} %pad_clamp_fusion.1) | copy-start | bytes 12292
  152.4 2.6 %copy-start.14 = (pred[8,8]{1,0:T(8,128)(4,1)S(1)}, pred[8,8]{1,0:T(8,128)(4,1)}, u32[]{:S(2)}) copy-start(pred[8,8]{1,0:T(8,128)(4,1)} %compare_and_fusion) | copy-start | bytes 196
  168.0 2.4 %copy-start = (bf16[512,128]{1,0:T(8,128)(2,1)S(1)}, bf16[512,128]{1,0:T(8,128)(2,1)}, u32[]{:S(2)}) copy-start(bf16[512,128]{1,0:T(8,128)(2,1)} %fusion.29) | copy-start | bytes 393220
Sparse Core Ops, SparseCore 0:
  8.9 26.6 all-gather.4
  93.7 21.9 all-gather.6
where the time goes:
time: 179 us; the launch traced here: 178 us
  blocking collectives  75.3 us (42%)
  local copies, waits for them, and re-layouts  43.4 us (24%)
  matrix products  19.4 us (11%)
  between operations  13.8 us (8%)
  waiting for transfers between devices  9.68 us (5%)
  other arithmetic  8.83 us (5%)
  starting transfers between devices  7.59 us (4%)
    all_gather x2, blocking collectives, layer(): lax.all_gather(gain, 'tp', axis=0, tiled=True)  22.2 us
    all_gather x2, blocking collectives, layer(): lax.all_gather(w_value, 'sp', axis=0, tiled=True)  18.8 us
    all_gather x2, blocking collectives, layer(): lax.all_gather(w_query, 'sp', axis=0, tiled=True)  17.9 us
    all_gather x2, blocking collectives, layer(): lax.all_gather(w_key, 'sp', axis=0, tiled=True)  16.5 us
    gather x6, local copies, waits for them, and re-layouts, one_row(): key_block = lax.dynamic_slice_in_dim(keys, local, 8, 0)[:, key_cols]  12.4 us
    gather x6, local copies, waits for them, and re-layouts, one_row(): value_block = lax.dynamic_slice_in_dim(values, local, 8, 0)[:, key_cols]  12.3 us
    gather x4, local copies, waits for them, and re-layouts, attend(): column_bias = table[:, :, column_offset]  12.1 us
    dot_general x2, matrix products, one_row(): jnp.einsum('jqhe,mjkhe->hjqmk', query_row, key_block, preferred_element_t...  9.08 us
  transfers between devices with their start and end apart: 6, of which 4 were waited for; matrix products, arithmetic and copies ran while one was open for 10% of the time, Pallas kernels for 0%

commit v1 on v0

--- a/solution.py
+++ b/solution.py
@@ -6,6 +6,27 @@
 
 GRID_W = 64
 epsilon = 1e-06
+
+
+def gather_around(x, axis, dim):
+    size, mine, span = (lax.axis_size(axis), lax.axis_index(axis), x.shape[dim])
+    right = [(i, (i + 1) % size) for i in range(size)]
+    backward = [(i, (i - 1) % size) for i in range(size)]
+    filled = jnp.zeros((*x.shape[:dim], size * span, *x.shape[dim + 1 :]), x.dtype)
+    filled = lax.dynamic_update_slice_in_dim(filled, x, mine * span, axis=dim)
+    from_left = from_right = x
+    halfway = size // 2
+    for step in range(1, halfway + 1):
+        from_left = lax.ppermute(from_left, axis, right)
+        filled = lax.dynamic_update_slice_in_dim(
+            filled, from_left, (mine - step) % size * span, axis=dim
+        )
+        if step < size - halfway:
+            from_right = lax.ppermute(from_right, axis, backward)
+            filled = lax.dynamic_update_slice_in_dim(
+                filled, from_right, (mine + step) % size * span, axis=dim
+            )
+    return filled
 
 
 def padded_2(block, sides, width):
@@ -77,7 +98,7 @@
     )
     pieces = (
         lax.all_gather(w_query, "sp", axis=0, tiled=True),
-        lax.all_gather(w_key, "sp", axis=0, tiled=True),
+        gather_around(w_key, "sp", 0),
         lax.all_gather(w_value, "sp", axis=0, tiled=True),
     )
     query, key_part, value_part = tuple(

time: 179 us -> 181 us (1.011)
  blocking collectives: 75.3 us -> 55.3 us
  starting transfers between devices: 7.59 us -> 18.3 us
  waiting for transfers between devices: 9.68 us -> 16.1 us
  local copies, waits for them, and re-layouts: 43.4 us -> 45.9 us
    all_gather x2 -> x0, blocking collectives: 16.5 us -> none  [layer(): lax.all_gather(w_key, 'sp', axis=0, tiled=True)]
    ppermute x0 -> x6, starting transfers between devices: none -> 10.5 us  [the longest x4 9.46 us: gather_around(): from_left = lax.ppermute(from_left, axis, right)]
    ppermute x0 -> x6, waiting for transfers between devices: none -> 6.21 us  [the longest x4 6.21 us: gather_around(): from_left = lax.ppermute(from_left, axis, right)]
    all_gather x2, blocking collectives: 17.9 us -> 15.8 us  [layer(): lax.all_gather(w_query, 'sp', axis=0, tiled=True)]
  transfers between devices with their start and end apart: 6 -> 12, of which waited for: 4 -> 6; matrix products, arithmetic and copies ran while one was open for 10% -> 12% of each run, Pallas kernels for 0% -> 0%
where the time goes in v1:
time: 181 us; the launch traced here: 179 us
  blocking collectives  55.3 us (31%)
  local copies, waits for them, and re-layouts  45.9 us (25%)
  matrix products  19.4 us (11%)
  starting transfers between devices  18.3 us (10%)
  waiting for transfers between devices  16.1 us (9%)
  between operations  13.8 us (8%)
  other arithmetic  10.4 us (6%)
    all_gather x2, blocking collectives, layer(): lax.all_gather(gain, 'tp', axis=0, tiled=True)  20.6 us
    all_gather x2, blocking collectives, layer(): lax.all_gather(w_value, 'sp', axis=0, tiled=True)  18.9 us
    all_gather x2, blocking collectives, layer(): lax.all_gather(w_query, 'sp', axis=0, tiled=True)  15.8 us
    gather x6, local copies, waits for them, and re-layouts, one_row(): key_block = lax.dynamic_slice_in_dim(keys, local, 8, 0)[:, key_cols]  12.4 us
    gather x6, local copies, waits for them, and re-layouts, one_row(): value_block = lax.dynamic_slice_in_dim(values, local, 8, 0)[:, key_cols]  12.2 us
    gather x4, local copies, waits for them, and re-layouts, attend(): column_bias = table[:, :, column_offset]  12.1 us
    ppermute x4, starting transfers between devices, gather_around(): from_left = lax.ppermute(from_left, axis, right)  9.46 us
    dot_general x2, matrix products, one_row(): jnp.einsum('jqhe,mjkhe->hjqmk', query_row, key_block, preferred_element_t...  9.08 us
  transfers between devices with their start and end apart: 12, of which 6 were waited for; matrix products, arithmetic and copies ran while one was open for 12% of the time, Pallas kernels for 0%

profile of v1, /device:TPU:0, one launch (start us, length us, event | category | flops | bytes accessed | tf_op | source)
XLA Modules:
  0.0 179.3 jit_solution(10947888615254876447)
XLA Ops:
  7.3 3.0 %collective-permute-start = (bf16[256,128]{1,0:T(8,128)(2,1)}, bf16[256,128]{1,0:T(8,128)(2,1)S(1)}, u32[]{:S(2)}, u32[]{:S(2)}) collective-permute-start(bf16[256,128]{1,0:T(8,128)(2,1)} %param.28), channel_id=1, source_target_pairs={{0,8},{8,16},{16,24},{24,0},{1,9},{9,17},{17,25},{25,1},{2,10},{10... | collective-permute-start | bytes 196616 | tf_op jit(solution)/shard_map/ppermute | solution.py:20
  15.0 9.4 %all_gather.26 = bf16[1024,128]{1,0:T(8,128)(2,1)S(1)} all-gather(bf16[256,128]{1,0:T(8,128)(2,1)} %param.29), channel_id=1, replica_groups=mesh['sp'=4,'tp'=8] {'sp'}, dimensions={0}, use_global_device_ids=true | all-gather | bytes 327680 | tf_op jit(solution)/shard_map/all_gather | solution.py:102
  24.4 12.1 %all-gather = bf16[8,1,128]{2,1,0:T(2,128)(2,1)S(1)} all-gather(bf16[1,1,128]{2,1,0:T(2,128)(2,1)} %bitcast.156), channel_id=1, replica_groups=mesh['sp'=4,'tp'=8] {'tp'}, dimensions={0}, use_global_device_ids=true | all-gather | bytes 2304 | tf_op jit(solution)/shard_map/all_gather | solution.py:92
  37.4 5.5 %gather_fusion.5 = f32[2048,15]{1,0:T(8,128)S(1)} fusion(f32[15,31]{0,1:T(8,128)S(1)} %bitcast.127, s32[2048]{0:T(1024)S(1)} %broadcast_clamp_fusion), kind=kCustom, calls=%fused_computation.7 | custom fusion | bytes 253952 | tf_op jit(solution)/shard_map/gather | solution.py:55
  44.3 8.3 %all_gather.27 = bf16[1024,128]{1,0:T(8,128)(2,1)S(1)} all-gather(bf16[256,128]{1,0:T(8,128)(2,1)S(1)} %copy-done.5), channel_id=1, replica_groups=mesh['sp'=4,'tp'=8] {'sp'}, dimensions={0}, use_global_device_ids=true | all-gather | bytes 327680 | tf_op jit(solution)/shard_map/all_gather | solution.py:100
  54.7 3.1 %collective-permute-done.2 = bf16[256,128]{1,0:T(8,128)(2,1)S(1)} collective-permute-done((bf16[256,128]{1,0:T(8,128)(2,1)S(1)}, bf16[256,128]{1,0:T(8,128)(2,1)S(1)}, u32[]{:S(2)}, u32[]{:S(2)}) %collective-permute-start.2) | collective-permute-done | bytes 65568 | tf_op jit(solution)/shard_map/ppermute | solution.py:20
  59.5 1.7 convolution_convert_fusion.5
  61.8 2.2 %collective-permute-start.3 = (bf16[2,4,64,1,128]{4,2,1,3,0:T(8,128)(2,1)S(1)}, bf16[2,4,64,1,128]{4,2,1,3,0:T(8,128)(2,1)S(1)}, u32[]{:S(2)}, u32[]{:S(2)}) collective-permute-start(bf16[2,4,64,1,128]{4,2,1,3,0:T(8,128)(2,1)S(1)} %get-tuple-element.12), channel_id=1, source_target_pairs={{0,8},{8,16},{16,24},{1,9},{9,17},{17,25},{2,10},{10,18},{18,26},{... | collective-permute-start | bytes 393224 | tf_op jit(solution)/shard_map/ppermute | solution.py:37
  67.1 4.2 %collective-permute-done.4 = bf16[2,4,64,1,128]{4,2,1,3,0:T(8,128)(2,1)} collective-permute-done((bf16[2,4,64,1,128]{4,2,1,3,0:T(8,128)(2,1)S(1)}, bf16[2,4,64,1,128]{4,2,1,3,0:T(8,128)(2,1)}, u32[]{:S(2)}, u32[]{:S(2)}) %collective-permute-start.4) | collective-permute-done | bytes 131104 | tf_op jit(solution)/shard_map/ppermute | solution.py:40
  72.4 1.7 gather_fusion.3
  74.0 1.9 %copy.56 = bf16[8,8,64,128]{3,1,2,0:T(8,128)(2,1)S(1)} copy(bf16[8,8,64,128]{3,2,1,0:T(8,128)(2,1)} %gather_fusion.3) | data formatting | bytes 2097152 | tf_op jit(solution)/shard_map/vmap()/gather | solution.py:63
  76.0 2.7 %gather_fusion.4 = bf16[128,8,8,128]{3,2,1,0:T(8,128)(2,1)} fusion(bf16[8,8,64,128]{3,1,2,0:T(8,128)(2,1)S(1)} %copy.56, s32[1024]{0:T(1024)} %pad_clamp_fusion.1), kind=kCustom, calls=%fused_computation.6 | custom fusion | bytes 4194816 | tf_op jit(solution)/shard_map/vmap()/gather | solution.py:63
  78.6 4.5 %fusion.39 = (f32[8,4,16]{2,1,0:T(4,128)S(1)}, f32[8,1,4,16,8,32]{5,3,4,2,0,1:T(8,128)S(1)}) fusion(f32[8,1,8,4,16,32]{5,4,3,2,0,1:T(8,128)S(1)} %bitcast.131, pred[8,8]{1,0:T(8,128)(4,1)} %compare_and_fusion, bf16[8,4,16,128,1]{3,2,4,1,0:T(8,128)(2,1)S(1)} %bitcast.139, bf16[4,32,8,8,128]{4,3,2,1,0:T(8,128)(2,1)} %bitcast.135, ...), kind=kOutput, calls=%fused_computation.95 | convolution fusion | flops 34209280 | bytes 3280960 | tf_op jit(solution)/shard_map/vmap(jqhe,mjkhe->hjqmk)/dot_general | solution.py:69
  87.2 1.9 %copy.52 = bf16[8,8,64,128]{3,1,2,0:T(8,128)(2,1)S(1)} copy(bf16[8,8,64,128]{3,2,1,0:T(8,128)(2,1)} %gather_fusion) | data formatting | bytes 2097152 | tf_op jit(solution)/shard_map/vmap()/gather | solution.py:64
  89.1 2.5 %gather_fusion.1 = bf16[128,8,8,128]{3,2,1,0:T(8,128)(2,1)} fusion(bf16[8,8,64,128]{3,1,2,0:T(8,128)(2,1)S(1)} %copy.52, s32[1024]{0:T(1024)S(1)} %copy-done.9), kind=kCustom, calls=%fused_computation.3 | custom fusion | bytes 4194816 | tf_op jit(solution)/shard_map/vmap()/gather | solution.py:64
  91.7 2.4 %fusion.14 = f32[8,4,128,16,1]{2,3,4,1,0:T(8,128)S(1)} fusion(bf16[8,4,16,8,32]{2,3,4,1,0:T(8,128)(2,1)S(1)} %copy.61, bf16[4,32,8,8,128]{4,3,2,1,0:T(8,128)(2,1)} %bitcast.133), kind=kOutput, calls=%fused_computation.34 | convolution fusion | flops 33554432 | bytes 2621440 | tf_op jit(solution)/shard_map/vmap(hjqmk,mjkhe->jqhe)/dot_general | solution.py:79
  94.9 3.1 %collective-permute-start.5 = (bf16[256,128]{1,0:T(8,128)(2,1)S(1)}, bf16[256,128]{1,0:T(8,128)(2,1)S(1)}, u32[]{:S(2)}, u32[]{:S(2)}) collective-permute-start(bf16[256,128]{1,0:T(8,128)(2,1)S(1)} %copy-done.8), channel_id=1, source_target_pairs={{0,8},{8,16},{16,24},{24,0},{1,9},{9,17},{17,25},{25,1},{2,10},{10... | collective-permute-start | bytes 196616 | tf_op jit(solution)/shard_map/ppermute | solution.py:20
  98.1 9.5 %all_gather.30 = bf16[1024,128]{1,0:T(8,128)(2,1)S(1)} all-gather(bf16[256,128]{1,0:T(8,128)(2,1)S(1)} %copy-done.6), channel_id=1, replica_groups=mesh['sp'=4,'tp'=8] {'sp'}, dimensions={0}, use_global_device_ids=true | all-gather | bytes 327680 | tf_op jit(solution)/shard_map/all_gather | solution.py:102
  107.6 8.4 %all-gather.1 = bf16[8,1,128]{2,1,0:T(2,128)(2,1)S(1)} all-gather(bf16[1,1,128]{2,1,0:T(2,128)(2,1)S(1)} %bitcast.157), channel_id=1, replica_groups=mesh['sp'=4,'tp'=8] {'tp'}, dimensions={0}, use_global_device_ids=true | all-gather | bytes 2304 | tf_op jit(solution)/shard_map/all_gather | solution.py:92
  116.1 5.5 %gather_fusion.11 = f32[2048,15]{1,0:T(8,128)S(1)} fusion(f32[15,31]{0,1:T(8,128)S(1)} %bitcast.126, s32[2048]{0:T(1024)S(1)} %broadcast_clamp_fusion), kind=kCustom, calls=%fused_computation.13 | custom fusion | bytes 253952 | tf_op jit(solution)/shard_map/gather | solution.py:55
  123.1 7.5 %all_gather.31 = bf16[1024,128]{1,0:T(8,128)(2,1)S(1)} all-gather(bf16[256,128]{1,0:T(8,128)(2,1)S(1)} %copy-done.7), channel_id=1, replica_groups=mesh['sp'=4,'tp'=8] {'sp'}, dimensions={0}, use_global_device_ids=true | all-gather | bytes 327680 | tf_op jit(solution)/shard_map/all_gather | solution.py:100
  130.6 2.1 %collective-permute-start.7 = (bf16[256,128]{1,0:T(8,128)(2,1)S(1)}, bf16[256,128]{1,0:T(8,128)(2,1)S(1)}, u32[]{:S(2)}, u32[]{:S(2)}) collective-permute-start(bf16[256,128]{1,0:T(8,128)(2,1)S(1)} %collective-permute-done.5), channel_id=1, source_target_pairs={{0,8},{8,16},{16,24},{24,0},{1,9},{9,17},{17,25},{25,1},{2,10},{10... | collective-permute-start | bytes 196616 | tf_op jit(solution)/shard_map/ppermute | solution.py:20
  132.7 3.1 %collective-permute-done.7 = bf16[256,128]{1,0:T(8,128)(2,1)S(1)} collective-permute-done((bf16[256,128]{1,0:T(8,128)(2,1)S(1)}, bf16[256,128]{1,0:T(8,128)(2,1)S(1)}, u32[]{:S(2)}, u32[]{:S(2)}) %collective-permute-start.7) | collective-permute-done | bytes 65568 | tf_op jit(solution)/shard_map/ppermute | solution.py:20
  137.5 1.7 convolution_convert_fusion.1
  139.8 3.0 %collective-permute-start.8 = (bf16[2,4,64,1,128]{4,2,1,3,0:T(8,128)(2,1)S(1)}, bf16[2,4,64,1,128]{4,2,1,3,0:T(8,128)(2,1)S(1)}, u32[]{:S(2)}, u32[]{:S(2)}) collective-permute-start(bf16[2,4,64,1,128]{4,2,1,3,0:T(8,128)(2,1)S(1)} %get-tuple-element.10), channel_id=1, source_target_pairs={{0,8},{8,16},{16,24},{1,9},{9,17},{17,25},{2,10},{10,18},{18,26},{... | collective-permute-start | bytes 393224 | tf_op jit(solution)/shard_map/ppermute | solution.py:37
  145.3 4.7 %collective-permute-done.9 = bf16[2,4,64,1,128]{4,2,1,3,0:T(8,128)(2,1)S(1)} collective-permute-done((bf16[2,4,64,1,128]{4,2,1,3,0:T(8,128)(2,1)S(1)}, bf16[2,4,64,1,128]{4,2,1,3,0:T(8,128)(2,1)S(1)}, u32[]{:S(2)}, u32[]{:S(2)}) %collective-permute-start.9) | collective-permute-done | bytes 131104 | tf_op jit(solution)/shard_map/ppermute | solution.py:40
  151.8 1.9 %copy.66 = bf16[8,8,64,128]{3,1,2,0:T(8,128)(2,1)S(1)} copy(bf16[8,8,64,128]{3,2,1,0:T(8,128)(2,1)} %gather_fusion.9) | data formatting | bytes 2097152 | tf_op jit(solution)/shard_map/vmap()/gather | solution.py:63
  153.7 2.5 %gather_fusion.10 = bf16[128,8,8,128]{3,2,1,0:T(8,128)(2,1)} fusion(bf16[8,8,64,128]{3,1,2,0:T(8,128)(2,1)S(1)} %copy.66, s32[1024]{0:T(1024)S(1)} %copy-done.10), kind=kCustom, calls=%fused_computation.12 | custom fusion | bytes 4194816 | tf_op jit(solution)/shard_map/vmap()/gather | solution.py:63
  156.3 4.5 %fusion.40 = (f32[8,4,16]{2,1,0:T(4,128)S(1)}, f32[8,1,4,16,8,32]{5,3,4,2,0,1:T(8,128)S(1)}) fusion(f32[8,1,8,4,16,32]{5,4,3,2,0,1:T(8,128)S(1)} %bitcast.130, pred[8,8]{1,0:T(8,128)(4,1)S(1)} %copy-done.13, bf16[8,4,16,128,1]{3,2,4,1,0:T(8,128)(2,1)S(1)} %bitcast.138, bf16[4,32,8,8,128]{4,3,2,1,0:T(8,128)(2,1)} %bitcast.134, ...), kind=kOutput, calls=%fused_computation.96 | convolution fusion | flops 34209280 | bytes 3280960 | tf_op jit(solution)/shard_map/vmap(jqhe,mjkhe->hjqmk)/dot_general | solution.py:69
  164.9 1.9 %copy.62 = bf16[8,8,64,128]{3,1,2,0:T(8,128)(2,1)S(1)} copy(bf16[8,8,64,128]{3,2,1,0:T(8,128)(2,1)} %gather_fusion.6) | data formatting | bytes 2097152 | tf_op jit(solution)/shard_map/vmap()/gather | solution.py:64
  166.8 2.5 %gather_fusion.7 = bf16[128,8,8,128]{3,2,1,0:T(8,128)(2,1)} fusion(bf16[8,8,64,128]{3,1,2,0:T(8,128)(2,1)S(1)} %copy.62, s32[1024]{0:T(1024)S(1)} %copy-done.10), kind=kCustom, calls=%fused_computation.9 | custom fusion | bytes 4194816 | tf_op jit(solution)/shard_map/vmap()/gather | solution.py:64
  169.3 2.4 %fusion.9 = f32[8,4,128,16,1]{2,3,4,1,0:T(8,128)S(1)} fusion(bf16[8,4,16,8,32]{2,3,4,1,0:T(8,128)(2,1)S(1)} %copy.71, bf16[4,32,8,8,128]{4,3,2,1,0:T(8,128)(2,1)} %bitcast.132), kind=kOutput, calls=%fused_computation.28 | convolution fusion | flops 33554432 | bytes 2621440 | tf_op jit(solution)/shard_map/vmap(hjqmk,mjkhe->jqhe)/dot_general | solution.py:79
  (103 shorter events, 33.7 us)
Async XLA Ops:
  6.5 51.3 %all-gather.5.cloned.1.call-start = ((), (), s32[]{:S(2)}) async-start(), calls=%async_computation | async-start | bytes 1179648 | tf_op jit(solution)/shard_map/all_gather | solution.py:91
  7.3 128.6 %all-gather.7.cloned.1.call-start = ((), (), s32[]{:S(2)}) async-start(), calls=%async_computation.1 | async-start | bytes 1179648 | tf_op jit(solution)/shard_map/all_gather | solution.py:91
  7.3 45.3 %collective-permute-start = (bf16[256,128]{1,0:T(8,128)(2,1)}, bf16[256,128]{1,0:T(8,128)(2,1)S(1)}, u32[]{:S(2)}, u32[]{:S(2)}) collective-permute-start(bf16[256,128]{1,0:T(8,128)(2,1)} %param.28), channel_id=1, source_target_pairs={{0,8},{8,16},{16,24},{24,0},{1,9},{9,17},{17,25},{25,1},{2,10},{10... | collective-permute-start | bytes 196616 | tf_op jit(solution)/shard_map/ppermute | solution.py:20
  10.3 43.6 %collective-permute-start.1 = (bf16[256,128]{1,0:T(8,128)(2,1)}, bf16[256,128]{1,0:T(8,128)(2,1)}, u32[]{:S(2)}, u32[]{:S(2)}) collective-permute-start(bf16[256,128]{1,0:T(8,128)(2,1)} %param.28), channel_id=1, source_target_pairs={{0,24},{8,0},{16,8},{24,16},{1,25},{9,1},{17,9},{25,17},{2,26},{10... | collective-permute-start | bytes 196616 | tf_op jit(solution)/shard_map/ppermute | solution.py:25
  12.8 30.7 %copy-start.11 = (s32[1024]{0:T(1024)}, s32[1024]{0:T(1024)S(1)}, u32[]{:S(2)}) copy-start(s32[1024]{0:T(1024)S(1)} %pad_clamp_fusion) | copy-start | bytes 12292
  43.5 0.8 copy-start.5
  52.6 5.2 %collective-permute-start.2 = (bf16[256,128]{1,0:T(8,128)(2,1)S(1)}, bf16[256,128]{1,0:T(8,128)(2,1)S(1)}, u32[]{:S(2)}, u32[]{:S(2)}) collective-permute-start(bf16[256,128]{1,0:T(8,128)(2,1)S(1)} %collective-permute-done), channel_id=1, source_target_pairs={{0,8},{8,16},{16,24},{24,0},{1,9},{9,17},{17,25},{25,1},{2,10},{10... | collective-permute-start | bytes 196616 | tf_op jit(solution)/shard_map/ppermute | solution.py:20
  57.9 3.3 %copy-start.1 = (bf16[512,1024]{1,0:T(8,128)(2,1)S(1)}, bf16[512,1024]{1,0:T(8,128)(2,1)}, u32[]{:S(2)}) copy-start(bf16[512,1024]{1,0:T(8,128)(2,1)} %all-gather.5.cloned.1.call-done) | copy-start | bytes 3145732
  61.8 4.7 %collective-permute-start.3 = (bf16[2,4,64,1,128]{4,2,1,3,0:T(8,128)(2,1)S(1)}, bf16[2,4,64,1,128]{4,2,1,3,0:T(8,128)(2,1)S(1)}, u32[]{:S(2)}, u32[]{:S(2)}) collective-permute-start(bf16[2,4,64,1,128]{4,2,1,3,0:T(8,128)(2,1)S(1)} %get-tuple-element.12), channel_id=1, source_target_pairs={{0,8},{8,16},{16,24},{1,9},{9,17},{17,25},{2,10},{10,18},{18,26},{... | collective-permute-start | bytes 393224 | tf_op jit(solution)/shard_map/ppermute | solution.py:37
  64.0 7.3 %collective-permute-start.4 = (bf16[2,4,64,1,128]{4,2,1,3,0:T(8,128)(2,1)S(1)}, bf16[2,4,64,1,128]{4,2,1,3,0:T(8,128)(2,1)}, u32[]{:S(2)}, u32[]{:S(2)}) collective-permute-start(bf16[2,4,64,1,128]{4,2,1,3,0:T(8,128)(2,1)S(1)} %get-tuple-element.13), channel_id=1, source_target_pairs={{8,0},{16,8},{24,16},{9,1},{17,9},{25,17},{10,2},{18,10},{26,18},{... | collective-permute-start | bytes 393224 | tf_op jit(solution)/shard_map/ppermute | solution.py:40
  66.5 0.7 copy-start.4
  85.5 3.6 %copy-start.9 = (s32[1024]{0:T(1024)S(1)}, s32[1024]{0:T(1024)}, u32[]{:S(2)}) copy-start(s32[1024]{0:T(1024)} %pad_clamp_fusion.1) | copy-start | bytes 12292
  91.7 2.5 %copy-start.3 = (bf16[512,128]{1,0:T(8,128)(2,1)S(1)}, bf16[512,128]{1,0:T(8,128)(2,1)}, u32[]{:S(2)}) copy-start(bf16[512,128]{1,0:T(8,128)(2,1)} %param.25) | copy-start | bytes 393220
  91.7 3.2 %copy-start.8 = (bf16[256,128]{1,0:T(8,128)(2,1)S(1)}, bf16[256,128]{1,0:T(8,128)(2,1)}, u32[]{:S(2)}) copy-start(bf16[256,128]{1,0:T(8,128)(2,1)} %param.33) | copy-start | bytes 196612
  91.7 6.4 %copy-start.6 = (bf16[256,128]{1,0:T(8,128)(2,1)S(1)}, bf16[256,128]{1,0:T(8,128)(2,1)}, u32[]{:S(2)}) copy-start(bf16[256,128]{1,0:T(8,128)(2,1)} %param.34) | copy-start | bytes 196612
  91.7 15.9 %copy-start.15 = (bf16[128]{0:T(256)(128)(2,1)S(1)}, bf16[128]{0:T(256)(128)(2,1)}, u32[]{:S(2)}) copy-start(bf16[128]{0:T(256)(128)(2,1)} %param.31) | copy-start | bytes 772
  91.7 24.4 %copy-start.14 = (f32[1,15,31]{2,0,1:T(1,128)S(1)}, f32[1,15,31]{2,0,1:T(1,128)}, u32[]{:S(2)}) copy-start(f32[1,15,31]{2,0,1:T(1,128)} %param.35) | copy-start | bytes 5584
  94.9 35.7 %collective-permute-start.5 = (bf16[256,128]{1,0:T(8,128)(2,1)S(1)}, bf16[256,128]{1,0:T(8,128)(2,1)S(1)}, u32[]{:S(2)}, u32[]{:S(2)}) collective-permute-start(bf16[256,128]{1,0:T(8,128)(2,1)S(1)} %copy-done.8), channel_id=1, source_target_pairs={{0,8},{8,16},{16,24},{24,0},{1,9},{9,17},{17,25},{25,1},{2,10},{10... | collective-permute-start | bytes 196616 | tf_op jit(solution)/shard_map/ppermute | solution.py:20
  98.0 34.7 %collective-permute-start.6 = (bf16[256,128]{1,0:T(8,128)(2,1)S(1)}, bf16[256,128]{1,0:T(8,128)(2,1)S(1)}, u32[]{:S(2)}, u32[]{:S(2)}) collective-permute-start(bf16[256,128]{1,0:T(8,128)(2,1)S(1)} %copy-done.8), channel_id=1, source_target_pairs={{0,24},{8,0},{16,8},{24,16},{1,25},{9,1},{17,9},{25,17},{2,26},{10... | collective-permute-start | bytes 196616 | tf_op jit(solution)/shard_map/ppermute | solution.py:25
  116.1 6.1 %copy-start.12 = (s32[1024]{0:T(1024)S(1)}, s32[1024]{0:T(1024)}, u32[]{:S(2)}) copy-start(s32[1024]{0:T(1024)} %copy-done.11) | copy-start | bytes 12292
  122.2 0.8 copy-start.7
  130.6 5.2 %collective-permute-start.7 = (bf16[256,128]{1,0:T(8,128)(2,1)S(1)}, bf16[256,128]{1,0:T(8,128)(2,1)S(1)}, u32[]{:S(2)}, u32[]{:S(2)}) collective-permute-start(bf16[256,128]{1,0:T(8,128)(2,1)S(1)} %collective-permute-done.5), channel_id=1, source_target_pairs={{0,8},{8,16},{16,24},{24,0},{1,9},{9,17},{17,25},{25,1},{2,10},{10... | collective-permute-start | bytes 196616 | tf_op jit(solution)/shard_map/ppermute | solution.py:20
  135.9 3.3 %copy-start.2 = (bf16[512,1024]{1,0:T(8,128)(2,1)S(1)}, bf16[512,1024]{1,0:T(8,128)(2,1)}, u32[]{:S(2)}) copy-start(bf16[512,1024]{1,0:T(8,128)(2,1)} %all-gather.7.cloned.1.call-done) | copy-start | bytes 3145732
  139.8 5.5 %collective-permute-start.8 = (bf16[2,4,64,1,128]{4,2,1,3,0:T(8,128)(2,1)S(1)}, bf16[2,4,64,1,128]{4,2,1,3,0:T(8,128)(2,1)S(1)}, u32[]{:S(2)}, u32[]{:S(2)}) collective-permute-start(bf16[2,4,64,1,128]{4,2,1,3,0:T(8,128)(2,1)S(1)} %get-tuple-element.10), channel_id=1, source_target_pairs={{0,8},{8,16},{16,24},{1,9},{9,17},{17,25},{2,10},{10,18},{18,26},{... | collective-permute-start | bytes 393224 | tf_op jit(solution)/shard_map/ppermute | solution.py:37
  142.8 7.2 %collective-permute-start.9 = (bf16[2,4,64,1,128]{4,2,1,3,0:T(8,128)(2,1)S(1)}, bf16[2,4,64,1,128]{4,2,1,3,0:T(8,128)(2,1)S(1)}, u32[]{:S(2)}, u32[]{:S(2)}) collective-permute-start(bf16[2,4,64,1,128]{4,2,1,3,0:T(8,128)(2,1)S(1)} %get-tuple-element.11), channel_id=1, source_target_pairs={{8,0},{16,8},{24,16},{9,1},{17,9},{25,17},{10,2},{18,10},{26,18},{... | collective-permute-start | bytes 393224 | tf_op jit(solution)/shard_map/ppermute | solution.py:40
  150.1 3.6 %copy-start.10 = (s32[1024]{0:T(1024)S(1)}, s32[1024]{0:T(1024)}, u32[]{:S(2)}) copy-start(s32[1024]{0:T(1024)} %pad_clamp_fusion.1) | copy-start | bytes 12292
  153.7 2.5 %copy-start.13 = (pred[8,8]{1,0:T(8,128)(4,1)S(1)}, pred[8,8]{1,0:T(8,128)(4,1)}, u32[]{:S(2)}) copy-start(pred[8,8]{1,0:T(8,128)(4,1)} %compare_and_fusion) | copy-start | bytes 196
  169.3 2.4 %copy-start = (bf16[512,128]{1,0:T(8,128)(2,1)S(1)}, bf16[512,128]{1,0:T(8,128)(2,1)}, u32[]{:S(2)}) copy-start(bf16[512,128]{1,0:T(8,128)(2,1)} %fusion.29) | copy-start | bytes 393220
Sparse Core Ops, SparseCore 0:
  8.9 26.8 all-gather.4
  95.0 22.5 all-gather.6
